TPU v7x, 32 devices: a whole 2x2x4 slice. The times are simulated.
32 devices in a mesh: sp: 8 (over z, x), tp: 4 (over y, core).
Axes of the slice: x: 2, y: 2, z: 4, core: 2. Of those that a mesh axis runs over, the one named last changes fastest.
Arguments:
- skip_stream_input: bfloat16 [1024, 2048], P('sp'), may hold values from -16 to 16
- asking_vectors_split: bfloat16 [1024, 2048], P('sp', 'tp'), may hold values from -8 to 8
- lookup_vectors_split: bfloat16 [1024, 512], P('sp'), may hold values from -8 to 8
- content_vectors_split: bfloat16 [1024, 512], P('sp'), may hold values from -6 to 6
- asking_rms_gain: float32 [128], replicated, may hold values from 0.1 to 1.9
- lookup_rms_gain: float32 [128], replicated, may hold values from 0.1 to 1.9
- softness_per_channel: float32 [16], P('tp'), may hold values from 1.5 to 24
- mixing_exit_weights: bfloat16 [2048, 2048], P('tp'), may hold values from -0.125 to 0.125
- specialist_rms_gain: float32 [2048], replicated, may hold values from 0.1 to 1.9
- selected_dispatch_weights: float32 [1024, 2], P('sp'), may hold values from -6 to 6
- selected_specialist_ids: int32 [1024, 2], P('sp'), may hold values from 0 to 7, all different within a row; in each aligned block of 128 rows (0 to 127, 128 to 255, ...) at most 48 rows name the same one
- specialist_switch_weights: bfloat16 [8, 2048, 2048], P('sp', None, 'tp'), may hold values from -0.125 to 0.125
- specialist_widen_weights: bfloat16 [8, 2048, 2048], P('sp', None, 'tp'), may hold values from -0.125 to 0.125
- specialist_shrink_weights: bfloat16 [8, 2048, 2048], P('sp', 'tp'), may hold values from -0.125 to 0.125
Outputs:
- layer_out: bfloat16 [1024, 2048], P('sp', 'tp')
Inputs may be any that keep to these rules, and one draw needn't show every extreme that they name: `selected_specialist_ids`: each row names 2 different experts. In each aligned block of 128 rows no expert is named by more than 48 rows, a bound that some block reaches.
All inputs are finite; a program needn't handle non-finite values.
Results may differ from a plain program's by a relative error of at most 0.0085.
Values may be sent and summed in bfloat16 or wider, within the bound.
A program may use at most 64 MiB of HBM per device.

v0:
```python
import math
import jax
import jax.numpy as jnp
from jax import lax
from jax.sharding import PartitionSpec as P

CHANNEL_WIDTH = 128
GROUP = 4
GRID_W = 64
EPSILON = 1e-06
NEGATIVE = -1e30


def rotate_half(values_in, positions, full_width):
    half_width = full_width // 2
    frequency = 10000.0 ** (-jnp.arange(half_width, dtype=jnp.float32) / half_width)
    angles = positions.astype(jnp.float32)[:, None] * frequency[None, :]
    cosine = jnp.cos(angles)[:, None, :]
    sine = jnp.sin(angles)[:, None, :]
    leading = values_in[..., :half_width]
    trailing = values_in[..., half_width:]
    return jnp.concatenate(
        [leading * cosine - trailing * sine, trailing * cosine + leading * sine], axis=-1
    )


def norm_rotate(heads_in, gain_vec, positions):
    widened = heads_in.astype(jnp.float32)
    scaled = (
        widened
        * lax.rsqrt(jnp.mean(widened * widened, axis=-1, keepdims=True) + EPSILON)
        * gain_vec
    )
    half_width = scaled.shape[-1] // 2
    grid_rows = positions // GRID_W
    grid_cols = positions % GRID_W
    turned = jnp.concatenate(
        [
            rotate_half(scaled[..., :half_width], grid_rows, half_width),
            rotate_half(scaled[..., half_width:], grid_cols, half_width),
        ],
        axis=-1,
    )
    return turned.astype(jnp.bfloat16)


def shards(
    skip_stream_input,
    asking_vectors_split,
    lookup_vectors_split,
    content_vectors_split,
    asking_rms_gain,
    lookup_rms_gain,
    softness_per_channel,
    mixing_exit_weights,
    specialist_rms_gain,
    selected_dispatch_weights,
    selected_specialist_ids,
    specialist_switch_weights,
    specialist_widen_weights,
    specialist_shrink_weights,
):
    tok_count = skip_stream_input.shape[0]
    model_width = skip_stream_input.shape[1]
    heads_here = asking_vectors_split.shape[1] // CHANNEL_WIDTH
    local_key_value_heads = max(1, heads_here // GROUP)
    local_group_count = heads_here // local_key_value_heads
    tp_position = lax.axis_index("tp")
    positions = lax.axis_index("sp") * tok_count + jnp.arange(tok_count, dtype=jnp.int32)
    query_turned = norm_rotate(
        asking_vectors_split.reshape(tok_count, heads_here, CHANNEL_WIDTH),
        asking_rms_gain,
        positions,
    )
    first_head = tp_position * heads_here // GROUP
    key_cols = lax.dynamic_slice_in_dim(
        lookup_vectors_split, first_head * CHANNEL_WIDTH, local_key_value_heads * CHANNEL_WIDTH, 1
    )
    value_cols = lax.dynamic_slice_in_dim(
        content_vectors_split, first_head * CHANNEL_WIDTH, local_key_value_heads * CHANNEL_WIDTH, 1
    )
    key_turned = norm_rotate(
        key_cols.reshape(tok_count, local_key_value_heads, CHANNEL_WIDTH),
        lookup_rms_gain,
        positions,
    )
    key_turned = key_turned.reshape(tok_count, local_key_value_heads * CHANNEL_WIDTH)
    query_grouped = query_turned.reshape(
        tok_count, local_key_value_heads, local_group_count, CHANNEL_WIDTH
    ).transpose(1, 2, 0, 3)
    inverse_root_width = (softness_per_channel / math.sqrt(CHANNEL_WIDTH)).reshape(
        local_key_value_heads, local_group_count, 1, 1
    )

    def absorb(run_state, key_span, value_span):
        run_max, run_sum, run_acc = run_state
        scores = (
            jnp.einsum(
                "kgqd,nkd->kgqn", query_grouped, key_span, preferred_element_type=jnp.float32
            )
            * inverse_root_width
        )
        new_max = jnp.maximum(run_max, jnp.max(scores, axis=-1))
        factor = jnp.exp(run_max - new_max)
        exp_terms = jnp.exp(scores - new_max[..., None])
        run_sum = run_sum * factor + jnp.sum(exp_terms, axis=-1)
        run_acc = run_acc * factor[..., None] + jnp.einsum(
            "kgqn,nkd->kgqd",
            exp_terms.astype(jnp.bfloat16),
            value_span,
            preferred_element_type=jnp.float32,
        )
        return (new_max, run_sum, run_acc)

    initial = (
        jnp.full((local_key_value_heads, local_group_count, tok_count), NEGATIVE, jnp.float32),
        jnp.zeros((local_key_value_heads, local_group_count, tok_count), jnp.float32),
        jnp.zeros(
            (local_key_value_heads, local_group_count, tok_count, CHANNEL_WIDTH), jnp.float32
        ),
    )
    key_piece = lax.all_gather(key_turned, "sp", axis=0, tiled=True)
    value_piece = lax.all_gather(value_cols, "sp", axis=0, tiled=True)
    piece_len = key_piece.shape[0]
    span_len = 1024
    span_count = piece_len // span_len
    key_spans = key_piece.reshape(span_count, span_len, local_key_value_heads, CHANNEL_WIDTH)
    value_spans = value_piece.reshape(span_count, span_len, local_key_value_heads, CHANNEL_WIDTH)

    def step_span(inner_state, span_pair):
        return (absorb(inner_state, span_pair[0], span_pair[1]), None)

    result_state, unused = lax.scan(step_span, initial, (key_spans, value_spans))
    final_max, final_sum, final_acc = result_state
    attn_heads = (final_acc / final_sum[..., None]).astype(jnp.bfloat16)
    attn_flat = attn_heads.transpose(2, 0, 1, 3).reshape(tok_count, heads_here * CHANNEL_WIDTH)
    partial_sum = jnp.dot(attn_flat, mixing_exit_weights, preferred_element_type=jnp.float32)
    share_width = model_width // lax.axis_size("tp")
    first_col = tp_position * share_width
    attended = lax.psum(partial_sum.astype(jnp.bfloat16), "tp")
    mid_rows = (skip_stream_input.astype(jnp.float32) + attended.astype(jnp.float32)).astype(
        jnp.bfloat16
    )
    mid_wide = mid_rows.astype(jnp.float32)
    normed_rows = (
        mid_wide
        * lax.rsqrt(jnp.mean(mid_wide * mid_wide, axis=-1, keepdims=True) + EPSILON)
        * specialist_rms_gain
    ).astype(jnp.bfloat16)
    mid_share = lax.dynamic_slice_in_dim(mid_rows, first_col, share_width, 1)
    outgoing_rows = lax.dynamic_slice_in_dim(normed_rows, first_col, share_width, 1)
    experts_count = lax.axis_size("sp")
    top_count = selected_specialist_ids.shape[1]
    capacity = max(2, 3 * tok_count * top_count // (2 * experts_count))
    flat_ids = selected_specialist_ids.reshape(-1)
    one_hot = (flat_ids[:, None] == jnp.arange(experts_count, dtype=jnp.int32)[None, :]).astype(
        jnp.int32
    )
    earlier = jnp.cumsum(one_hot, axis=0) - one_hot
    slot_index = jnp.sum(earlier * one_hot, axis=1)
    destination = flat_ids * capacity + slot_index
    owner_rows = jnp.arange(tok_count * top_count, dtype=jnp.int32) // top_count
    slot_owner = jnp.zeros((experts_count * capacity,), jnp.int32).at[destination].set(owner_rows)
    filled = jnp.zeros((experts_count * capacity,), jnp.int32).at[destination].set(1)
    outgoing = jnp.where(
        filled[:, None] > 0, outgoing_rows[slot_owner], jnp.zeros((), jnp.bfloat16)
    )
    outgoing = outgoing.reshape(experts_count, capacity, outgoing_rows.shape[1])
    gate_local = specialist_switch_weights[0]
    up_local = specialist_widen_weights[0]
    down_local = specialist_shrink_weights[0]
    arrived = lax.all_to_all(outgoing, "sp", split_axis=0, concat_axis=0, tiled=True)
    row_count = arrived.shape[0] * arrived.shape[1]
    feature_piece = lax.all_gather(arrived, "tp", axis=2, tiled=True)
    piece_width = feature_piece.shape[2]
    flat_piece = feature_piece.reshape(row_count, piece_width)
    gate_acc = jnp.dot(flat_piece, gate_local, preferred_element_type=jnp.float32)
    up_acc = jnp.dot(flat_piece, up_local, preferred_element_type=jnp.float32)
    hidden = (jax.nn.silu(gate_acc) * up_acc).astype(jnp.bfloat16)
    expert_part = jnp.dot(hidden, down_local, preferred_element_type=jnp.float32)
    expert_part = expert_part.reshape(arrived.shape[0], arrived.shape[1], model_width)
    expert_share = lax.psum_scatter(
        expert_part.astype(jnp.bfloat16), "tp", scatter_dimension=2, tiled=True
    )
    returned = lax.all_to_all(expert_share, "sp", split_axis=0, concat_axis=0, tiled=True)
    back_flat = returned.reshape(experts_count * capacity, share_width)
    picked = back_flat[destination].reshape(tok_count, top_count, share_width).astype(jnp.float32)
    route_weights = jax.nn.softmax(selected_dispatch_weights, axis=-1)
    layer_out = mid_share.astype(jnp.float32) + jnp.sum(route_weights[..., None] * picked, axis=1)
    return layer_out.astype(jnp.bfloat16)


def solution(mesh):
    in_specs = (
        P("sp", None),
        P("sp", "tp"),
        P("sp", None),
        P("sp", None),
        P(),
        P(),
        P("tp"),
        P("tp", None),
        P(),
        P("sp", None),
        P("sp", None),
        P("sp", None, "tp"),
        P("sp", None, "tp"),
        P("sp", "tp", None),
    )
    out_specs = P("sp", "tp")
    return jax.shard_map(shards, mesh=mesh, in_specs=in_specs, out_specs=out_specs, check_vma=False)
```

profile of v0, /device:TPU:0, one launch (start us, length us, event | category | flops | bytes accessed | tf_op | source)
XLA Modules:
  0.0 204.7 jit_solution(4723165117829957611)
XLA Ops:
  6.5 0.0 copy-start
  6.5 0.0 all-reduce.2.cloned.1.call-start
  6.6 0.9 constant_dynamic-slice_fusion.1
  7.5 0.1 copy.35
  7.7 0.7 fusion.35
  8.4 0.5 multiply_cosine_fusion.1
  9.0 0.2 fusion.55
  9.2 28.3 %all_gather.9 = bf16[1024,128]{0,1:T(8,128)(2,1)S(1)} all-gather(bf16[128,128]{0,1:T(8,128)(2,1)S(1)} %pad_maximum_fusion), channel_id=1, replica_groups=mesh['sp'=8,'tp'=4] {'sp'}, dimensions={0}, use_global_device_ids=true | all-gather | bytes 294912 | tf_op jit(solution)/shard_map/all_gather | solution.py:122
  37.5 1.0 copy.24
  38.6 0.1 copy.25
  38.7 0.7 broadcast_multiply_fusion.1
  39.4 0.8 multiply_multiply_fusion
  40.2 0.3 fusion.23
  40.5 0.6 multiply_reduce_fusion
  41.1 1.3 copy-done.1
  42.4 0.5 fusion.5
  42.9 0.8 constant_dynamic-slice_fusion
  43.7 0.1 copy.36
  43.8 0.0 copy-start.2
  43.8 26.8 %all_gather.10 = bf16[1024,128]{0,1:T(8,128)(2,1)S(1)} all-gather(bf16[128,128]{0,1:T(8,128)(2,1)S(1)} %copy.36), channel_id=1, replica_groups=mesh['sp'=8,'tp'=4] {'sp'}, dimensions={0}, use_global_device_ids=true | all-gather | bytes 294912 | tf_op jit(solution)/shard_map/all_gather | solution.py:123
  70.7 2.2 %fusion.14 = bf16[4,128,128]{1,2,0:T(8,128)(2,1)S(1)} fusion(f32[4,128,1024]{2,1,0:T(8,128)} %copy-done.1, f32[4,128]{1,0:T(4,128)S(1)} %broadcast_maximum_fusion, f32[4]{0:T(128)S(1)} %broadcast_multiply_fusion.1, bf16[1024,128]{0,1:T(8,128)(2,1)S(1)} %all_gather.10, f32[4,128]{1,0:T(4,128)S(1)} %get-tuple-element.44, f32[4,128]{1,0:T(4,128)S(1)} %get-tuple-element.43), kind=kOutput, calls=%fused_computation.19 | convolution fusion | flops 135987200 | bytes 2496528 | tf_op jit(solution)/shard_map/while/body/eval_jaxpr/kgqn,nkd->kgqd/dot_general | solution.py:107
  72.9 0.0 copy-start.5
  72.9 0.0 copy-start.3
  72.9 0.0 copy-done.2
  72.9 1.3 convolution_convert_fusion.1
  74.2 0.0 all-reduce.2.cloned.1.call-update
  74.2 0.0 all-gather.2.cloned.1.call-start
  74.3 0.0 copy-done.5
  74.3 0.1 copy.31
  74.4 0.1 eq.32
  74.5 0.1 eq.28
  74.7 0.6 reduce-window.6
  75.3 0.2 slice_reduce_fusion
  75.5 0.1 copy.30
  75.7 0.1 mul.356
  75.8 0.1 fusion.53
  75.9 1.4 scatter_custom_fusion.1
  77.3 1.4 scatter_custom_fusion
  78.7 0.1 broadcast_in_dim.23
  78.8 0.8 dynamic-slice
  79.6 25.8 %all-reduce.2.cloned.1.call-done = bf16[128,2048]{1,0:T(8,128)(2,1)} async-done(((bf16[128,2048]{1,0:T(8,128)(2,1)}), bf16[128,2048]{1,0:T(8,128)(2,1)}) %all-reduce.2.cloned.1.call-update) | async-done | bytes 524304 | tf_op jit(solution)/shard_map/psum | solution.py:140
  105.4 0.0 copy-done.3
  105.4 1.3 multiply_reduce_fusion.1
  106.7 0.1 convert_element_type.107
  106.8 0.1 fusion.19
  106.9 2.1 %gather_fusion = bf16[384,512]{1,0:T(8,128)(2,1)S(1)} fusion(bf16[128,512]{1,0:T(8,128)(2,1)S(1)} %fusion.19, s32[1024]{0:T(1024)S(1)} %pad_clamp_fusion.1), kind=kCustom, calls=%fused_computation | custom fusion | bytes 787968 | tf_op jit(solution)/shard_map/gather | solution.py:166
  109.0 0.1 broadcast_select_fusion
  109.1 16.5 %all_to_all.10 = bf16[8,48,512]{2,1,0:T(8,128)(2,1)} all-to-all(bf16[8,48,512]{2,1,0:T(8,128)(2,1)S(1)} %broadcast_select_fusion), channel_id=1, replica_groups=mesh['sp'=8,'tp'=4] {'sp'}, dimensions={0} | all-to-all | bytes 786432 | tf_op jit(solution)/shard_map/all_to_all | solution.py:172
  125.6 0.0 all-gather.2.cloned.1.call-update
  125.6 0.0 reduce-scatter.2.cloned.1.call-start
  125.7 18.0 %all-gather.2.cloned.1.call-done = bf16[8,48,2048]{2,1,0:T(8,128)(2,1)} async-done(((bf16[8,48,512]{2,1,0:T(8,128)(2,1)}), bf16[8,48,2048]{2,1,0:T(8,128)(2,1)}) %all-gather.2.cloned.1.call-update) | async-done | bytes 1572880 | tf_op jit(solution)/shard_map/all_gather | solution.py:174
  143.7 3.2 %fusion.3 = f32[384,512]{1,0:T(8,128)S(1)} fusion(bf16[384,2048]{1,0:T(8,128)(2,1)} %bitcast.82, bf16[1,2048,512]{2,1,0:T(8,128)(2,1)} %param.25), kind=kOutput, calls=%fused_computation.9 | convolution fusion | flops 805306368 | bytes 4456448 | tf_op jit(solution)/shard_map/dot_general | solution.py:177
  146.9 1.0 fusion.10
  147.9 2.1 %convolution_convert_fusion = bf16[8,48,2048]{2,1,0:T(8,128)(2,1)} fusion(bf16[8,48,512]{2,1,0:T(8,128)(2,1)S(1)} %bitcast.84, bf16[1,512,2048]{2,1,0:T(8,128)(2,1)S(1)} %copy-done), kind=kOutput, calls=%fused_computation.4 | convolution fusion | flops 806092800 | bytes 4063232 | tf_op jit(solution)/shard_map/dot_general | solution.py:180
  150.0 0.0 reduce-scatter.2.cloned.1.call-update
  150.1 28.1 %reduce-scatter.2.cloned.1.call-done = bf16[8,48,512]{2,1,0:T(8,128)(2,1)} async-done(((bf16[8,48,2048]{2,1,0:T(8,128)(2,1)}), bf16[8,48,512]{2,1,0:T(8,128)(2,1)}) %reduce-scatter.2.cloned.1.call-update) | async-done | bytes 393232 | tf_op jit(solution)/shard_map/reduce_scatter | solution.py:182
  178.2 5.5 %all-to-all-start.1 = ((bf16[8,48,512]{2,1,0:T(8,128)(2,1)}), bf16[8,48,512]{2,1,0:T(8,128)(2,1)S(1)}, u32[]{:S(2)}, u32[]{:S(2)}) async-start(bf16[8,48,512]{2,1,0:T(8,128)(2,1)} %reduce-scatter.2.cloned.1.call-done), calls=%async_computation.2 | async-start | bytes 786432 | tf_op jit(solution)/shard_map/all_to_all | solution.py:185
  183.7 0.0 copy-done.4
  183.8 0.1 copy.29
  183.9 11.4 %all-to-all-done.1 = bf16[8,48,512]{2,1,0:T(8,128)(2,1)S(1)} async-done(((bf16[8,48,512]{2,1,0:T(8,128)(2,1)}), bf16[8,48,512]{2,1,0:T(8,128)(2,1)S(1)}, u32[]{:S(2)}, u32[]{:S(2)}) %all-to-all-start.1) | async-done | bytes 393248 | tf_op jit(solution)/shard_map/all_to_all | solution.py:185
  195.3 1.2 gather_fusion.1
  196.4 0.3 reshape.493
  196.8 0.7 multiply_reduce_fusion.2
  197.5 0.7 add_convert_fusion.1
  (31 shorter events, 0.3 us)
Async XLA Ops:
  6.5 141.4 %copy-start = (bf16[1,512,2048]{2,1,0:T(8,128)(2,1)S(1)}, bf16[1,512,2048]{2,1,0:T(8,128)(2,1)}, u32[]{:S(2)}) copy-start(bf16[1,512,2048]{2,1,0:T(8,128)(2,1)} %param.27) | copy-start | bytes 6291460
  6.5 98.8 %all-reduce.2.cloned.1.call-start = ((), (), s32[]{:S(2)}) async-start(), calls=%async_computation.3 | async-start | bytes 1048576 | tf_op jit(solution)/shard_map/psum | solution.py:140
  41.1 1.4 copy-start.1
  43.8 29.1 %copy-start.2 = (bf16[512,2048]{1,0:T(8,128)(2,1)S(1)}, bf16[512,2048]{1,0:T(8,128)(2,1)}, u32[]{:S(2)}) copy-start(bf16[512,2048]{1,0:T(8,128)(2,1)} %param.21) | copy-start | bytes 6291460
  72.9 1.4 copy-start.5
  72.9 32.5 %copy-start.3 = (bf16[128,2048]{1,0:T(8,128)(2,1)S(1)}, bf16[128,2048]{1,0:T(8,128)(2,1)}, u32[]{:S(2)}) copy-start(bf16[128,2048]{1,0:T(8,128)(2,1)} %param.14) | copy-start | bytes 1572868
  74.2 69.4 %all-gather.2.cloned.1.call-start = ((), (), s32[]{:S(2)}) async-start(), calls=%async_computation.4 | async-start | bytes 1966080 | tf_op jit(solution)/shard_map/all_gather | solution.py:174
  125.6 52.6 %reduce-scatter.2.cloned.1.call-start = ((), (), s32[]{:S(2)}) async-start(), calls=%async_computation.5 | async-start | bytes 1966080 | tf_op jit(solution)/shard_map/reduce_scatter | solution.py:182
  143.7 3.2 %copy-start.6 = (bf16[1,2048,512]{2,1,0:T(8,128)(2,1)S(1)}, bf16[1,2048,512]{2,1,0:T(8,128)(2,1)}, u32[]{:S(2)}) copy-start(bf16[1,2048,512]{2,1,0:T(8,128)(2,1)} %param.26) | copy-start | bytes 6291460
  143.7 3.2 %copy-start.7 = (bf16[8,48,2048]{2,1,0:T(8,128)(2,1)S(1)}, bf16[8,48,2048]{2,1,0:T(8,128)(2,1)}, u32[]{:S(2)}) copy-start(bf16[8,48,2048]{2,1,0:T(8,128)(2,1)} %all-gather.2.cloned.1.call-done) | copy-start | bytes 4718596
  150.0 33.7 %copy-start.4 = (f32[128,2]{0,1:T(2,128)S(1)}, f32[128,2]{0,1:T(2,128)}, u32[]{:S(2)}) copy-start(f32[128,2]{0,1:T(2,128)} %param.23) | copy-start | bytes 3076
  178.2 17.1 %all-to-all-start.1 = ((bf16[8,48,512]{2,1,0:T(8,128)(2,1)}), bf16[8,48,512]{2,1,0:T(8,128)(2,1)S(1)}, u32[]{:S(2)}, u32[]{:S(2)}) async-start(bf16[8,48,512]{2,1,0:T(8,128)(2,1)} %reduce-scatter.2.cloned.1.call-done), calls=%async_computation.2 | async-start | bytes 786432 | tf_op jit(solution)/shard_map/all_to_all | solution.py:185
Sparse Core Ops, SparseCore 0:
  74.3 30.9 all-reduce.1
  125.8 17.8 all-gather.1
  150.2 27.9 reduce-scatter.1
where the time goes:
time: 205 us
  waiting for transfers between devices  83.3 us (41%)
  blocking collectives  71.7 us (35%)
  between operations  13.5 us (7%)
  local copies, waits for them, and re-layouts  12.6 us (6%)
  matrix products  10.4 us (5%)
  other arithmetic  7.66 us (4%)
  starting transfers between devices  5.57 us (3%)
    all_gather x1, blocking collectives, shards(): key_piece = lax.all_gather(key_turned, 'sp', axis=0, tiled=True)  28.3 us
    reduce_scatter x1, waiting for transfers between devices, shards(): lax.psum_scatter(expert_part.astype(jnp.bfloat16), 'tp', scatter_dimensio...  28.1 us
    all_gather x1, blocking collectives, shards(): value_piece = lax.all_gather(value_cols, 'sp', axis=0, tiled=True)  26.8 us
    psum x1, waiting for transfers between devices, shards(): attended = lax.psum(partial_sum.astype(jnp.bfloat16), 'tp')  25.8 us
    all_gather x1, waiting for transfers between devices, shards(): feature_piece = lax.all_gather(arrived, 'tp', axis=2, tiled=True)  18 us
    all_to_all x1, blocking collectives, shards(): lax.all_to_all(outgoing, 'sp', split_axis=0, concat_axis=0, tiled=True)  16.5 us
    all_to_all x1, waiting for transfers between devices, shards(): lax.all_to_all(expert_share, 'sp', split_axis=0, concat_axis=0, tiled=True)  11.4 us
    all_to_all x1, starting transfers between devices, shards(): lax.all_to_all(expert_share, 'sp', split_axis=0, concat_axis=0, tiled=True)  5.48 us
  transfers between devices with their start and end apart: 4, of which 4 were waited for; matrix products, arithmetic and copies ran while one was open for 3% of the time, Pallas kernels for 0%

commit v1 on v0

--- a/solution.py
+++ b/solution.py
@@ -171,7 +171,8 @@
     down_local = specialist_shrink_weights[0]
     arrived = lax.all_to_all(outgoing, "sp", split_axis=0, concat_axis=0, tiled=True)
     row_count = arrived.shape[0] * arrived.shape[1]
-    feature_piece = lax.all_gather(arrived, "tp", axis=2, tiled=True)
+    blocks = lax.all_gather(arrived, "tp")
+    feature_piece = jnp.concatenate(blocks, axis=2)
     piece_width = feature_piece.shape[2]
     flat_piece = feature_piece.reshape(row_count, piece_width)
     gate_acc = jnp.dot(flat_piece, gate_local, preferred_element_type=jnp.float32)

time: 205 us -> 208 us (1.015)
  local copies, waits for them, and re-layouts: 12.6 us -> 17.4 us
  matrix products: 10.4 us -> 8.21 us
    reshape x0 -> x1, local copies, waits for them, and re-layouts: none -> 2.63 us  [shards(): feature_piece = jnp.concatenate(blocks, axis=2)]
    dot_general x1, matrix products: 3.18 us -> 0.99 us  [shards(): jnp.dot(flat_piece, gate_local, preferred_element_type=jnp.float32)]
    unnamed x20 -> x21, local copies, waits for them, and re-layouts: 2.73 us -> 4.9 us
where the time goes in v1:
time: 208 us; the launch traced here: 207 us
  waiting for transfers between devices  83.3 us (40%)
  blocking collectives  71.7 us (34%)
  local copies, waits for them, and re-layouts  17.4 us (8%)
  between operations  13.5 us (6%)
  matrix products  8.21 us (4%)
  other arithmetic  7.66 us (4%)
  starting transfers between devices  5.57 us (3%)
    all_gather x1, blocking collectives, shards(): key_piece = lax.all_gather(key_turned, 'sp', axis=0, tiled=True)  28.3 us
    reduce_scatter x1, waiting for transfers between devices, shards(): lax.psum_scatter(expert_part.astype(jnp.bfloat16), 'tp', scatter_dimensio...  28.1 us
    all_gather x1, blocking collectives, shards(): value_piece = lax.all_gather(value_cols, 'sp', axis=0, tiled=True)  26.8 us
    psum x1, waiting for transfers between devices, shards(): attended = lax.psum(partial_sum.astype(jnp.bfloat16), 'tp')  25.8 us
    all_gather x1, waiting for transfers between devices, shards(): blocks = lax.all_gather(arrived, 'tp')  18 us
    all_to_all x1, blocking collectives, shards(): lax.all_to_all(outgoing, 'sp', split_axis=0, concat_axis=0, tiled=True)  16.5 us
    all_to_all x1, waiting for transfers between devices, shards(): lax.all_to_all(expert_share, 'sp', split_axis=0, concat_axis=0, tiled=True)  11.4 us
    all_to_all x1, starting transfers between devices, shards(): lax.all_to_all(expert_share, 'sp', split_axis=0, concat_axis=0, tiled=True)  5.48 us
  transfers between devices with their start and end apart: 4, of which 4 were waited for; matrix products, arithmetic and copies ran while one was open for 3% of the time, Pallas kernels for 0%

profile of v1, /device:TPU:0, one launch (start us, length us, event | category | flops | bytes accessed | tf_op | source)
XLA Modules:
  0.0 207.3 jit_solution(14964391127555685979)
XLA Ops:
  6.5 0.0 copy-start
  6.6 0.9 constant_dynamic-slice_fusion.1
  7.5 0.1 copy.52
  7.7 0.7 fusion.35
  8.4 0.5 multiply_cosine_fusion.1
  9.0 0.2 fusion.55
  9.2 28.3 %all_gather.12 = bf16[1024,128]{0,1:T(8,128)(2,1)S(1)} all-gather(bf16[128,128]{0,1:T(8,128)(2,1)S(1)} %pad_maximum_fusion), channel_id=1, replica_groups=mesh['sp'=8,'tp'=4] {'sp'}, dimensions={0}, use_global_device_ids=true | all-gather | bytes 294912 | tf_op jit(solution)/shard_map/all_gather | solution.py:122
  37.5 1.0 copy.40
  38.6 0.1 copy.41
  38.7 0.7 broadcast_multiply_fusion.1
  39.4 0.8 multiply_multiply_fusion
  40.2 0.3 fusion.23
  40.5 0.6 multiply_reduce_fusion
  41.1 1.3 copy-done.1
  42.4 0.5 fusion.5
  42.9 0.8 constant_dynamic-slice_fusion
  43.7 0.1 copy.53
  43.8 0.0 copy-start.2
  43.8 26.8 %all_gather.13 = bf16[1024,128]{0,1:T(8,128)(2,1)S(1)} all-gather(bf16[128,128]{0,1:T(8,128)(2,1)S(1)} %copy.53), channel_id=1, replica_groups=mesh['sp'=8,'tp'=4] {'sp'}, dimensions={0}, use_global_device_ids=true | all-gather | bytes 294912 | tf_op jit(solution)/shard_map/all_gather | solution.py:123
  70.7 2.2 %fusion.14 = bf16[4,128,128]{1,2,0:T(8,128)(2,1)S(1)} fusion(f32[4,128,1024]{2,1,0:T(8,128)} %copy-done.1, f32[4,128]{1,0:T(4,128)S(1)} %broadcast_maximum_fusion, f32[4]{0:T(128)S(1)} %broadcast_multiply_fusion.1, bf16[1024,128]{0,1:T(8,128)(2,1)S(1)} %all_gather.13, f32[4,128]{1,0:T(4,128)S(1)} %get-tuple-element.44, f32[4,128]{1,0:T(4,128)S(1)} %get-tuple-element.43), kind=kOutput, calls=%fused_computation.19 | convolution fusion | flops 135987200 | bytes 2496528 | tf_op jit(solution)/shard_map/while/body/eval_jaxpr/kgqn,nkd->kgqd/dot_general | solution.py:107
  72.9 0.0 copy-start.5
  72.9 0.0 copy-start.3
  72.9 1.3 convolution_convert_fusion.1
  74.2 0.0 all-reduce.2.cloned.1.call-update
  74.2 0.0 all-gather.3.cloned.1.call-start
  74.3 0.1 copy.47
  74.4 0.1 eq.32
  74.5 0.1 eq.28
  74.7 0.6 reduce-window.6
  75.3 0.2 slice_reduce_fusion
  75.5 0.1 copy.46
  75.7 0.1 mul.356
  75.8 0.1 fusion.53
  75.9 1.4 scatter_custom_fusion.1
  77.3 1.4 scatter_custom_fusion
  78.7 0.1 broadcast_in_dim.23
  78.8 0.8 dynamic-slice
  79.6 25.8 %all-reduce.2.cloned.1.call-done = bf16[128,2048]{1,0:T(8,128)(2,1)} async-done(((bf16[128,2048]{1,0:T(8,128)(2,1)}), bf16[128,2048]{1,0:T(8,128)(2,1)}) %all-reduce.2.cloned.1.call-update) | async-done | bytes 524304 | tf_op jit(solution)/shard_map/psum | solution.py:140
  105.4 1.3 multiply_reduce_fusion.1
  106.7 0.1 convert_element_type.107
  106.8 0.1 fusion.19
  106.9 2.1 gather_fusion
  109.0 0.1 broadcast_select_fusion
  109.1 16.5 %all_to_all.10 = bf16[8,48,512]{2,1,0:T(8,128)(2,1)} all-to-all(bf16[8,48,512]{2,1,0:T(8,128)(2,1)S(1)} %broadcast_select_fusion), channel_id=1, replica_groups=mesh['sp'=8,'tp'=4] {'sp'}, dimensions={0} | all-to-all | bytes 786432 | tf_op jit(solution)/shard_map/all_to_all | solution.py:172
  125.6 0.0 all-gather.3.cloned.1.call-update
  125.6 0.0 reduce-scatter.2.cloned.1.call-start
  125.7 18.0 %all-gather.3.cloned.1.call-done = bf16[32,48,512]{2,1,0:T(8,128)(2,1)} async-done(((bf16[8,48,512]{2,1,0:T(8,128)(2,1)}), bf16[32,48,512]{2,1,0:T(8,128)(2,1)}) %all-gather.3.cloned.1.call-update) | async-done | bytes 1572880 | tf_op jit(solution)/shard_map/all_gather | solution.py:174
  143.7 2.6 %copy.49 = bf16[8,48,4,512]{3,2,1,0:T(4,128)(2,1)S(1)} copy(bf16[8,48,4,512]{3,1,0,2:T(8,128)(2,1)} %bitcast.81) | data formatting | bytes 3145728 | tf_op jit(solution)/shard_map/reshape | solution.py:175
  146.3 0.0 copy-start.6
  146.3 0.4 copy.54
  146.7 1.1 copy-done.6
  147.9 1.0 fusion.3
  148.9 0.6 copy-done.7
  149.5 1.0 fusion.10
  150.5 2.1 %convolution_convert_fusion = bf16[8,48,2048]{2,1,0:T(8,128)(2,1)} fusion(bf16[8,48,512]{2,1,0:T(8,128)(2,1)S(1)} %bitcast.91, bf16[1,512,2048]{2,1,0:T(8,128)(2,1)S(1)} %copy-done), kind=kOutput, calls=%fused_computation.4 | convolution fusion | flops 806092800 | bytes 4063232 | tf_op jit(solution)/shard_map/dot_general | solution.py:181
  152.6 0.0 reduce-scatter.2.cloned.1.call-update
  152.7 28.1 %reduce-scatter.2.cloned.1.call-done = bf16[8,48,512]{2,1,0:T(8,128)(2,1)} async-done(((bf16[8,48,2048]{2,1,0:T(8,128)(2,1)}), bf16[8,48,512]{2,1,0:T(8,128)(2,1)}) %reduce-scatter.2.cloned.1.call-update) | async-done | bytes 393232 | tf_op jit(solution)/shard_map/reduce_scatter | solution.py:183
  180.8 5.5 %all-to-all-start.1 = ((bf16[8,48,512]{2,1,0:T(8,128)(2,1)}), bf16[8,48,512]{2,1,0:T(8,128)(2,1)S(1)}, u32[]{:S(2)}, u32[]{:S(2)}) async-start(bf16[8,48,512]{2,1,0:T(8,128)(2,1)} %reduce-scatter.2.cloned.1.call-done), calls=%async_computation.2 | async-start | bytes 786432 | tf_op jit(solution)/shard_map/all_to_all | solution.py:186
  186.4 0.1 copy.45
  186.5 11.4 %all-to-all-done.1 = bf16[8,48,512]{2,1,0:T(8,128)(2,1)S(1)} async-done(((bf16[8,48,512]{2,1,0:T(8,128)(2,1)}), bf16[8,48,512]{2,1,0:T(8,128)(2,1)S(1)}, u32[]{:S(2)}, u32[]{:S(2)}) %all-to-all-start.1) | async-done | bytes 393248 | tf_op jit(solution)/shard_map/all_to_all | solution.py:186
  197.9 1.2 gather_fusion.1
  199.0 0.3 reshape.493
  199.4 0.7 multiply_reduce_fusion.2
  200.1 0.7 add_convert_fusion.1
  (33 shorter events, 0.3 us)
Async XLA Ops:
  6.5 144.0 %copy-start = (bf16[1,512,2048]{2,1,0:T(8,128)(2,1)S(1)}, bf16[1,512,2048]{2,1,0:T(8,128)(2,1)}, u32[]{:S(2)}) copy-start(bf16[1,512,2048]{2,1,0:T(8,128)(2,1)} %param.27) | copy-start | bytes 6291460
  6.5 98.8 %all-reduce.2.cloned.1.call-start = ((), (), s32[]{:S(2)}) async-start(), calls=%async_computation.3 | async-start | bytes 1048576 | tf_op jit(solution)/shard_map/psum | solution.py:140
  41.1 1.4 copy-start.1
  43.8 29.1 %copy-start.2 = (bf16[512,2048]{1,0:T(8,128)(2,1)S(1)}, bf16[512,2048]{1,0:T(8,128)(2,1)}, u32[]{:S(2)}) copy-start(bf16[512,2048]{1,0:T(8,128)(2,1)} %param.21) | copy-start | bytes 6291460
  72.9 1.4 copy-start.5
  72.9 32.5 %copy-start.3 = (bf16[128,2048]{1,0:T(8,128)(2,1)S(1)}, bf16[128,2048]{1,0:T(8,128)(2,1)}, u32[]{:S(2)}) copy-start(bf16[128,2048]{1,0:T(8,128)(2,1)} %param.14) | copy-start | bytes 1572868
  74.2 69.4 %all-gather.3.cloned.1.call-start = ((), (), s32[]{:S(2)}) async-start(), calls=%async_computation.5 | async-start | bytes 1966080 | tf_op jit(solution)/shard_map/all_gather | solution.py:174
  125.6 55.2 %reduce-scatter.2.cloned.1.call-start = ((), (), s32[]{:S(2)}) async-start(), calls=%async_computation.4 | async-start | bytes 1966080 | tf_op jit(solution)/shard_map/reduce_scatter | solution.py:183
  146.3 1.6 copy-start.6
  147.9 1.6 copy-start.7
  152.6 33.7 %copy-start.4 = (f32[128,2]{0,1:T(2,128)S(1)}, f32[128,2]{0,1:T(2,128)}, u32[]{:S(2)}) copy-start(f32[128,2]{0,1:T(2,128)} %param.23) | copy-start | bytes 3076
  180.8 17.1 %all-to-all-start.1 = ((bf16[8,48,512]{2,1,0:T(8,128)(2,1)}), bf16[8,48,512]{2,1,0:T(8,128)(2,1)S(1)}, u32[]{:S(2)}, u32[]{:S(2)}) async-start(bf16[8,48,512]{2,1,0:T(8,128)(2,1)} %reduce-scatter.2.cloned.1.call-done), calls=%async_computation.2 | async-start | bytes 786432 | tf_op jit(solution)/shard_map/all_to_all | solution.py:186
Sparse Core Ops, SparseCore 0:
  74.3 30.9 all-reduce.1
  125.8 17.8 all-gather.2
  152.8 27.9 reduce-scatter.1
